TPU v7x, 32 devices: a whole 2x2x4 slice. The times are simulated.
32 devices in a mesh: ep: 16 (over z, y, core), tp: 2 (over x).
Axes of the slice: x: 2, y: 2, z: 4, core: 2. Of those that a mesh axis runs over, the one named last changes fastest.
Arguments:
- tokens: bfloat16 [288, 1024], P('ep'), may hold values from -16 to 16
- delta_state: float32 [288, 4, 128, 128], P('ep', 'tp'), may hold values from -1.8 to 1.8
- mixer_gain: float32 [1024], replicated, may hold values from 0.1 to 1.9
- query_weight: bfloat16 [1024, 512], P(None, 'tp'), may hold values from -0.1875 to 0.1875
- key_weight: bfloat16 [1024, 512], P(None, 'tp'), may hold values from -0.1875 to 0.1875
- value_weight: bfloat16 [1024, 512], P(None, 'tp'), may hold values from -0.1875 to 0.1875
- write_weight: bfloat16 [1024, 4], P(None, 'tp'), may hold values from -0.1875 to 0.1875
- decay_weight: bfloat16 [1024, 4], P(None, 'tp'), may hold values from -0.1875 to 0.1875
- decay_rate: float32 [4], P('tp'), may hold values from 0.05 to 4
- decay_bias: float32 [4], P('tp'), may hold values from -2 to 1
- head_gain: float32 [128], replicated, may hold values from 0.1 to 1.9
- out_weight: bfloat16 [512, 1024], P('tp'), may hold values from -0.25 to 0.25
- channel_gain: float32 [1024], replicated, may hold values from 0.1 to 1.9
- routes: int32 [288, 6], P('ep'), may hold values from 0 to 15, all different within a row; in each aligned block of 18 rows (0 to 17, 18 to 35, ...) at most 13 rows name the same one
- route_weights: float32 [288, 6], P('ep'), may hold values from 0.1 to 1
- expert_gate: bfloat16 [16, 1024, 512], P('ep', None, 'tp'), may hold values from -0.1875 to 0.1875
- expert_up: bfloat16 [16, 1024, 512], P('ep', None, 'tp'), may hold values from -0.1875 to 0.1875
- expert_down: bfloat16 [16, 512, 1024], P('ep', 'tp'), may hold values from -0.25 to 0.25
- shared_gate: bfloat16 [1024, 512], P(None, 'tp'), may hold values from -0.1875 to 0.1875
- shared_up: bfloat16 [1024, 512], P(None, 'tp'), may hold values from -0.1875 to 0.1875
- shared_down: bfloat16 [512, 1024], P('tp'), may hold values from -0.25 to 0.25
Outputs:
- layer_out: bfloat16 [288, 1024], P('ep', 'tp')
- next_state: float32 [288, 4, 128, 128], P('ep', 'tp')
Inputs may be any that keep to these rules, and one draw needn't show every extreme that they name: `routes`: each row names 6 different experts. In each aligned block of 18 rows (the rows of one ep index) no expert is named by more than 13 rows, a bound that some block reaches.
All inputs are finite; a program needn't handle non-finite values.
Results may differ from a plain program's by a relative error of at most 0.015.
Values may be sent and summed in bfloat16 or wider, within the bound.
A program may use at most 64 MiB of HBM per device.

v0:
```python
import functools

import jax
import jax.numpy as jnp
from jax import lax
from jax.experimental import pallas as pl
from jax.experimental.pallas import tpu as pltpu
from jax.sharding import PartitionSpec as P

EPS = 1e-06
ROUTED_SCALE = 2.5
MESH = pl.DeviceIdType.MESH
F32 = jnp.float32
BF16 = jnp.bfloat16


def rms_rows(values, gain_row):
    mean_square = jnp.mean(values * values, axis=-1, keepdims=True)
    return values * lax.rsqrt(mean_square + EPS) * gain_row


def round_up(value, step):
    return -(-value // step) * step


def mixer_kernel(
    expert_total, chunk,
    tokens_ref, mixer_gain_ref, write_ref, decay_ref, rate_ref, bias_ref,
    head_gain_ref, routes_ref, route_weights_ref,
    state_hbm, query_hbm, key_hbm, value_hbm, out_hbm,
    next_hbm, partial_ref, wext_ref,
    state, query_w, key_w, value_w, out_w, columns, readout, spread,
    weight_sems, in_sems, out_sems,
):
    rows, heads, dim = state.shape[0], state.shape[1], state.shape[2]
    chunks = rows // chunk
    weights = [
        pltpu.make_async_copy(src, dst, weight_sems.at[i])
        for i, (src, dst) in enumerate(
            ((key_hbm, key_w), (query_hbm, query_w), (value_hbm, value_w), (out_hbm, out_w))
        )
    ]
    loads = [
        pltpu.make_async_copy(
            state_hbm.at[pl.ds(i * chunk, chunk)], state.at[pl.ds(i * chunk, chunk)], in_sems.at[i]
        )
        for i in range(chunks)
    ]
    stores = [
        pltpu.make_async_copy(
            state.at[pl.ds(i * chunk, chunk)], next_hbm.at[pl.ds(i * chunk, chunk)], out_sems.at[i]
        )
        for i in range(chunks)
    ]
    for copy in weights[:3] + loads + weights[3:]:
        copy.start()

    raw = route_weights_ref[...]
    norm = raw / jnp.sum(raw, axis=0, keepdims=True) * ROUTED_SCALE
    routes = routes_ref[...]
    row = lax.broadcasted_iota(jnp.int32, (spread.shape[0], rows), 0)
    high = jnp.zeros(row.shape, F32)
    for k in range(routes.shape[0]):
        named = routes[k : k + 1, :]
        hit = (row == named) | (row == named + expert_total)
        high = high + jnp.where(hit, norm[k : k + 1, :], 0.0)
    rounded = high.astype(BF16).astype(F32)
    spread[:, :rows] = jnp.where(row < expert_total, rounded, high - rounded)
    wext_ref[...] = spread[...].T[:rows, :].astype(BF16)

    normed = rms_rows(tokens_ref[...].astype(F32), mixer_gain_ref[...]).astype(BF16)
    wide = normed.astype(F32)

    def per_head_dot(ref):
        table = ref[...].astype(F32)
        return [jnp.sum(wide * table[h : h + 1, :], axis=-1, keepdims=True) for h in range(heads)]

    write_rate = [jax.nn.sigmoid(x) for x in per_head_dot(write_ref)]
    keep = []
    for h, pre in enumerate(per_head_dot(decay_ref)):
        pre = pre + bias_ref[:, h : h + 1]
        softplus = jnp.maximum(pre, 0.0) + jnp.log1p(jnp.exp(-jnp.abs(pre)))
        keep.append(jnp.exp(-rate_ref[:, h : h + 1] * softplus))

    def project(copy, ref):
        copy.wait()
        return jnp.dot(normed, ref[...], preferred_element_type=F32).astype(BF16).astype(F32)

    key_raw = project(weights[0], key_w)
    query_raw = project(weights[1], query_w)
    value_raw = project(weights[2], value_w)
    stride = round_up(rows, 8)
    per_head = []
    for h in range(heads):
        part = slice(h * dim, (h + 1) * dim)
        k_h, q_h = key_raw[:, part], query_raw[:, part]
        k_h = k_h * lax.rsqrt(jnp.sum(k_h * k_h, axis=-1, keepdims=True) + EPS)
        q_h = q_h * lax.rsqrt(jnp.sum(q_h * q_h, axis=-1, keepdims=True) + EPS) * dim ** (-0.5)
        columns[2 * h * stride : 2 * h * stride + rows, :] = k_h
        columns[(2 * h + 1) * stride : (2 * h + 1) * stride + rows, :] = q_h
        dots = jnp.sum(k_h * q_h, axis=-1, keepdims=True)
        per_head.append(
            (
                value_raw[:, part],
                jnp.broadcast_to(keep[h], (rows, dim)),
                jnp.broadcast_to(write_rate[h], (rows, dim)),
                jnp.broadcast_to(dots, (rows, dim)),
            )
        )
    turned = columns[...].T

    for i in range(chunks):
        loads[i].wait()
        for r in range(i * chunk, (i + 1) * chunk):
            for h in range(heads):
                v_h, keep_h, write_h, dots_h = (x[r : r + 1, :] for x in per_head[h])
                at = 2 * h * stride + r
                k_col = jnp.broadcast_to(turned[:, at : at + 1], (dim, dim))
                q_col = jnp.broadcast_to(turned[:, at + stride : at + stride + 1], (dim, dim))
                old = state[r, h]
                seen = jnp.sum(old * k_col, axis=0, keepdims=True)
                asked = jnp.sum(old * q_col, axis=0, keepdims=True)
                step = write_h * (v_h - keep_h * seen)
                state[r, h] = keep_h * old + k_col * step
                readout[r : r + 1, h * dim : (h + 1) * dim] = keep_h * asked + dots_h * step
        stores[i].start()

    weights[3].wait()
    total = jnp.zeros(partial_ref.shape, F32)
    for h in range(heads):
        part = slice(h * dim, (h + 1) * dim)
        head_out = rms_rows(readout[:, part], head_gain_ref[...]).astype(BF16)
        total = total + jnp.dot(head_out, out_w[part, :], preferred_element_type=F32)
    partial_ref[...] = total.astype(BF16)
    for copy in stores:
        copy.wait()


def flip(index, mask):
    bit = 1
    while bit <= mask:
        if mask & bit:
            index = index + bit - 2 * bit * ((index // bit) % 2)
        bit *= 2
    return index


def experts_kernel(
    zs, ys, tps, pad,
    tokens_ref, partial_ref, wext_ref, channel_gain_ref,
    gate_hbm, up_hbm, down_hbm, sgate_hbm, sup_hbm, sdown_hbm,
    out_ref,
    gate_w, up_w, down_w, sgate_w, sup_w, sdown_w,
    mixed, blocks, packed, near, core_send, core_recv, y_send, y_recv,
    z_send, z_recv, own_share,
    weight_sems, x_send_sems, x_recv_sems,
    agz_send_sems, agz_recv_sems, agy_send_sems, agy_recv_sems,
    agc_send_sems, agc_recv_sems,
    rsc_send_sems, rsc_recv_sems, rsy_send_sems, rsy_recv_sems,
    rsz_send_sems, rsz_recv_sems,
):
    rows, width = tokens_ref.shape
    share = width // tps
    me, tp = lax.axis_index("ep"), lax.axis_index("tp")
    core, chip = me % 2, me // 2
    y, z = chip % ys, chip // ys
    expert_total = 2 * ys * zs

    def ep_of(dz, dy, dc):
        return (flip(z, dz) * ys + flip(y, dy)) * 2 + flip(core, dc)

    weights = [
        pltpu.make_async_copy(src, dst, weight_sems.at[i])
        for i, (src, dst) in enumerate(
            (
                (sgate_hbm, sgate_w), (sup_hbm, sup_w), (sdown_hbm, sdown_w),
                (gate_hbm, gate_w), (up_hbm, up_w), (down_hbm, down_w),
            )
        )
    ]
    for copy in weights:
        copy.start()

    peers = [(ep_of(dz, 0, 0), flip(tp, dt)) for dz in range(zs) for dt in range(tps) if dz or dt]
    peers += [(ep_of(0, dy, 0), tp) for dy in range(1, ys)] + [(ep_of(0, 0, 1), tp)]
    barrier = pltpu.get_barrier_semaphore()
    for peer in peers:
        pl.semaphore_signal(barrier, inc=1, device_id=peer, device_id_type=MESH)
    pl.semaphore_wait(barrier, len(peers))

    def remote(src, dst, send_sem, recv_sem, peer):
        copy = pltpu.make_async_remote_copy(
            src_ref=src, dst_ref=dst, send_sem=send_sem, recv_sem=recv_sem,
            device_id=peer, device_id_type=MESH,
        )
        copy.start()
        return copy

    sent = []

    x_copies = [
        remote(partial_ref, mixed.at[dt - 1], x_send_sems.at[dt - 1], x_recv_sems.at[dt - 1],
               (me, flip(tp, dt)))
        for dt in range(1, tps)
    ]
    mixer_out = partial_ref[...].astype(F32)
    for dt in range(1, tps):
        x_copies[dt - 1].wait_recv()
        mixer_out = mixer_out + mixed[dt - 1].astype(F32)
    sent += x_copies
    mixer_out = mixer_out.astype(BF16).astype(F32)
    residual = (tokens_ref[...].astype(F32) + mixer_out).astype(BF16)
    expert_input = rms_rows(residual.astype(F32), channel_gain_ref[...]).astype(BF16)
    for t in range(tps):
        own_share[t] = residual[:, t * share : (t + 1) * share].astype(F32)
    blocks[0, :, :width] = expert_input
    blocks[0, :, width:] = wext_ref[...]

    def slot(dz, dy, dc):
        return (dz * 2 + dc) * ys + dy

    order = [0] + list(range(zs - 1, 0, -1))
    z_copies = {
        dz: remote(blocks.at[slot(0, 0, 0)], blocks.at[slot(dz, 0, 0)],
                   agz_send_sems.at[dz], agz_recv_sems.at[dz], (ep_of(dz, 0, 0), tp))
        for dz in order[1:]
    }
    y_copies, c_copies = {}, {}

    def to_core(dz, dy):
        at = dz * ys + dy
        c_copies[dz, dy] = remote(
            blocks.at[slot(dz, dy, 0)], blocks.at[slot(dz, dy, 1)],
            agc_send_sems.at[at], agc_recv_sems.at[at], (ep_of(0, 0, 1), tp))

    def pack(dz, dy, dc):
        at = slot(dz, dy, dc)
        packed[at * pad : at * pad + rows, :] = blocks[at]

    def pass_on(dz):
        for dy in range(1, ys):
            at = dz * ys + dy
            y_copies[dz, dy] = remote(
                blocks.at[slot(dz, 0, 0)], blocks.at[slot(dz, dy, 0)],
                agy_send_sems.at[at], agy_recv_sems.at[at], (ep_of(0, dy, 0), tp))
        to_core(dz, 0)

    pass_on(0)

    for copy in weights[:3]:
        copy.wait()

    def gated(x, g_ref, u_ref):
        g = jnp.dot(x, g_ref[...], preferred_element_type=F32)
        u = jnp.dot(x, u_ref[...], preferred_element_type=F32)
        return (g * jax.nn.sigmoid(g) * u).astype(BF16)

    shared_act = gated(expert_input, sgate_w, sup_w)
    shared_part = jnp.dot(shared_act, sdown_w[...], preferred_element_type=F32)
    for copy in weights[3:]:
        copy.wait()

    def gather_z(dz):
        if dz:
            z_copies[dz].wait_recv()
            pass_on(dz)
        pack(dz, 0, 0)

    def gather_y(dz):
        for dy in range(1, ys):
            y_copies[dz, dy].wait_recv()
            to_core(dz, dy)
            pack(dz, dy, 0)

    half = ys * pad
    c_returns, y_returns, z_returns = {}, {}, []

    def run_expert(dz):
        for dy in range(ys):
            c_copies[dz, dy].wait_recv()
            pack(dz, dy, 1)
        first = slot(dz, 0, 0) * pad
        x = packed[first : first + 2 * half, :width]
        act = gated(x, gate_w, up_w)
        down = jnp.dot(act, down_w[...], preferred_element_type=F32)
        spread = packed[first : first + 2 * half, width:].astype(F32)
        lane = lax.broadcasted_iota(jnp.int32, spread.shape, 1)
        mine = (lane == me) | (lane == me + expert_total)
        down = down * jnp.sum(jnp.where(mine, spread, 0.0), axis=1, keepdims=True)
        for dy in range(ys - 1, -1, -1):
            n = dz * ys + dy
            core_send[n] = down[half + dy * pad : half + dy * pad + rows, :].astype(BF16)
            c_returns[n] = remote(core_send.at[n], core_recv.at[n], rsc_send_sems.at[n],
                                  rsc_recv_sems.at[n], (ep_of(0, 0, 1), tp))
        near[dz * half : (dz + 1) * half, :] = down[:half, :]

    def both_cores(dz, dy):
        n = dz * ys + dy
        c_returns[n].wait_recv()
        return near[n * pad : n * pad + rows, :] + core_recv[n].astype(F32)

    def return_y(dz):
        for dy in range(1, ys):
            n = dz * ys + dy
            y_send[n] = both_cores(dz, dy).astype(BF16)
            y_returns[n] = remote(y_send.at[n], y_recv.at[n], rsy_send_sems.at[n],
                                  rsy_recv_sems.at[n], (ep_of(0, dy, 0), tp))

    def return_z(dz):
        total = both_cores(dz, 0)
        for dy in range(1, ys):
            y_returns[dz * ys + dy].wait_recv()
            total = total + y_recv[dz * ys + dy].astype(F32)
        if dz == 0:
            total = total + shared_part
            for t in range(tps):
                own_share[t] = own_share[t] + total[:, t * share : (t + 1) * share]
        for t in range(tps):
            z_send[dz * tps + t] = total[:, t * share : (t + 1) * share].astype(BF16)
        for dt in range(tps - 1, -1, -1):
            if dz or dt:
                at = dz * tps + dt
                z_returns.append((at, remote(
                    z_send.at[dz * tps + flip(tp, dt)], z_recv.at[at],
                    rsz_send_sems.at[at], rsz_recv_sems.at[at],
                    (ep_of(dz, 0, 0), flip(tp, dt)))))

    stages = (gather_z, gather_y, run_expert, return_y, return_z)
    for step in range(zs + len(stages) - 1):
        for lag, stage in enumerate(stages):
            if 0 <= step - lag < zs:
                stage(order[step - lag])
    result = own_share[tp]
    for at, copy in z_returns:
        copy.wait_recv()
        result = result + z_recv[at].astype(F32)
    out_ref[...] = result.astype(BF16)

    sent += list(z_copies.values()) + list(y_copies.values()) + list(c_copies.values())
    sent += list(c_returns.values()) + list(y_returns.values()) + [copy for _, copy in z_returns]
    for copy in sent:
        copy.wait_send()


def per_device(
    ep_count, tp_count,
    tokens, delta_state, mixer_gain, query_weight, key_weight, value_weight,
    write_weight, decay_weight, decay_rate, decay_bias, head_gain, out_weight,
    channel_gain, routes, route_weights, expert_gate, expert_up, expert_down,
    shared_gate, shared_up, shared_down,
):
    rows, width = tokens.shape
    heads, dim = delta_state.shape[1], delta_state.shape[2]
    hidden = expert_gate.shape[2]
    shidden = shared_gate.shape[1]
    chips = ep_count // 2
    ys = 1
    while 4 * ys * ys <= chips:
        ys *= 2
    zs = chips // ys
    extra = round_up(2 * ep_count, 128)
    share = width // tp_count
    vmem = pl.BlockSpec(memory_space=pltpu.VMEM)
    anyspace = pl.BlockSpec(memory_space=pl.ANY)
    dma = pltpu.SemaphoreType.DMA
    chunk = next(c for c in (3, 2, 1) if rows % c == 0)
    column_rows = round_up(2 * heads * round_up(rows, 8), 128)

    next_state, partial, wext = pl.pallas_call(
        functools.partial(mixer_kernel, ep_count, chunk),
        out_shape=(
            jax.ShapeDtypeStruct(delta_state.shape, F32),
            jax.ShapeDtypeStruct((rows, width), BF16),
            jax.ShapeDtypeStruct((rows, extra), BF16),
        ),
        in_specs=[vmem] * 9 + [anyspace] * 5,
        out_specs=(anyspace, vmem, vmem),
        scratch_shapes=[
            pltpu.VMEM(delta_state.shape, F32),
            pltpu.VMEM(query_weight.shape, BF16),
            pltpu.VMEM(key_weight.shape, BF16),
            pltpu.VMEM(value_weight.shape, BF16),
            pltpu.VMEM(out_weight.shape, BF16),
            pltpu.VMEM((column_rows, dim), F32),
            pltpu.VMEM((rows, heads * dim), F32),
            pltpu.VMEM((extra, round_up(rows, 128)), F32),
            dma((4,)), dma((rows // chunk,)), dma((rows // chunk,)),
        ],
    )(
        tokens, mixer_gain.reshape(1, width), write_weight.T, decay_weight.T,
        decay_rate.reshape(1, heads), decay_bias.reshape(1, heads), head_gain.reshape(1, dim),
        routes.T, route_weights.T, delta_state, query_weight, key_weight, value_weight, out_weight,
    )

    pad = round_up(rows, 16)
    zy = zs * ys
    layer_out = pl.pallas_call(
        functools.partial(experts_kernel, zs, ys, tp_count, pad),
        out_shape=jax.ShapeDtypeStruct((rows, share), BF16),
        in_specs=[vmem] * 4 + [anyspace] * 6,
        out_specs=vmem,
        scratch_shapes=[
            pltpu.VMEM((width, hidden), BF16), pltpu.VMEM((width, hidden), BF16),
            pltpu.VMEM((hidden, width), BF16),
            pltpu.VMEM((width, shidden), BF16), pltpu.VMEM((width, shidden), BF16),
            pltpu.VMEM((shidden, width), BF16),
            pltpu.VMEM((max(1, tp_count - 1), rows, width), BF16),
            pltpu.VMEM((2 * zy, rows, width + extra), BF16),
            pltpu.VMEM((2 * zy * pad, width + extra), BF16),
            pltpu.VMEM((zy * pad, width), F32),
            pltpu.VMEM((zy, rows, width), BF16), pltpu.VMEM((zy, rows, width), BF16),
            pltpu.VMEM((zy, rows, width), BF16), pltpu.VMEM((zy, rows, width), BF16),
            pltpu.VMEM((zs * tp_count, rows, share), BF16),
            pltpu.VMEM((zs * tp_count, rows, share), BF16),
            pltpu.VMEM((tp_count, rows, share), F32),
            dma((6,)), dma((tp_count,)), dma((tp_count,)),
            dma((zs,)), dma((zs,)), dma((zy,)), dma((zy,)), dma((zy,)), dma((zy,)),
            dma((zy,)), dma((zy,)), dma((zy,)), dma((zy,)),
            dma((zs * tp_count,)), dma((zs * tp_count,)),
        ],
        compiler_params=pltpu.CompilerParams(collective_id=0, has_side_effects=True),
    )(
        tokens, partial, wext, channel_gain.reshape(1, width),
        expert_gate.reshape(width, hidden), expert_up.reshape(width, hidden),
        expert_down.reshape(hidden, width), shared_gate, shared_up, shared_down,
    )
    return layer_out, next_state


def solution(mesh):
    return jax.shard_map(
        functools.partial(per_device, mesh.shape["ep"], mesh.shape["tp"]),
        mesh=mesh,
        in_specs=(
            P("ep", None),
            P("ep", "tp", None, None),
            P(),
            P(None, "tp"),
            P(None, "tp"),
            P(None, "tp"),
            P(None, "tp"),
            P(None, "tp"),
            P("tp"),
            P("tp"),
            P(),
            P("tp", None),
            P(),
            P("ep", None),
            P("ep", None),
            P("ep", None, "tp"),
            P("ep", None, "tp"),
            P("ep", "tp", None),
            P(None, "tp"),
            P(None, "tp"),
            P("tp", None),
        ),
        out_specs=(P("ep", "tp"), P("ep", "tp", None, None)),
        check_vma=False,
    )
```

profile of v0, /device:TPU:0, one launch (start us, length us, event | category | flops | bytes accessed | tf_op | source)
XLA Modules:
  0.0 40.8 jit_solution(12543279571326582641)
XLA Ops:
  0.6 6.5 %shard_map.212 = (f32[18,2,128,128]{3,2,1,0:T(8,128)}, bf16[18,1024]{1,0:T(8,128)(2,1)}, bf16[18,128]{1,0:T(8,128)(2,1)}) custom-call(bf16[18,1024]{1,0:T(8,128)(2,1)} %tokens_ref.3, f32[1,1024]{1,0:T(1,128)} %bitcast.15, bf16[2,1024]{1,0:T(2,128)(2,1)} %bitcast.16, bf16[2,1024]{1,0:T(2,128)(2,1)} %bitcast.17, f32[1,2]{1,0:T(1,128)} %bitcast.21, ...), custom_call_target="tpu_custom_call" | custom-call | tf_op jit(solution)/shard_map/pallas_call | solution.py:369
  7.2 32.2 %shard_map.213 = bf16[18,512]{1,0:T(8,128)(2,1)} custom-call(bf16[18,1024]{1,0:T(8,128)(2,1)} %tokens_ref.3, bf16[18,1024]{1,0:T(8,128)(2,1)} %get-tuple-element.5.partial_ref, bf16[18,128]{1,0:T(8,128)(2,1)} %get-tuple-element.6.wext_ref, f32[1,1024]{1,0:T(1,128)} %bitcast.20, bf16[1024,256]{1,0:T(8,128)(2,1)} %bitcast.12, bf16[1024,256]{1,0:T(8,128)(2,1)} %bitcast.13, ...), custom_call_target="tpu_custom_call" | custom-call | tf_op jit(solution)/shard_map/pallas_call | solution.py:397
  39.4 1.3 %copy.24 = bf16[18,512]{1,0:T(8,128)(2,1)} copy(bf16[18,512]{1,0:T(8,128)(2,1)} %shard_map.213) | data formatting | bytes 36864
where the time goes:
time: 41.1 us; the launch traced here: 40.8 us
  Pallas kernels  38.8 us (94%)
  local copies, waits for them, and re-layouts  1.35 us (3%)
  between operations  0.65 us (2%)
    pallas_call x1, Pallas kernels, per_device(): pl.pallas_call(functools.partial(experts_kernel, zs, ys, tp_count, pad),...  32.2 us
    pallas_call x1, Pallas kernels, per_device(): pl.pallas_call(functools.partial(mixer_kernel, ep_count, chunk), out_shap...  6.54 us
    unnamed x1, local copies, waits for them, and re-layouts  1.35 us

commit v1 on v0

v1 whole, which is shorter than its diff:
```python
import functools

import jax
import jax.numpy as jnp
from jax import lax
from jax.experimental import pallas as pl
from jax.experimental.pallas import tpu as pltpu
from jax.sharding import PartitionSpec as P

EPS = 1e-06
ROUTED_SCALE = 2.5
MESH = pl.DeviceIdType.MESH
F32 = jnp.float32
BF16 = jnp.bfloat16


def rms_rows(values, gain_row):
    mean_square = jnp.mean(values * values, axis=-1, keepdims=True)
    return values * lax.rsqrt(mean_square + EPS) * gain_row


def round_up(value, step):
    return -(-value // step) * step


def flip(index, mask):
    bit = 1
    while bit <= mask:
        if mask & bit:
            index = index + bit - 2 * bit * ((index // bit) % 2)
        bit *= 2
    return index


def layer_kernel(
    zs, ys, tps, pad,
    tokens_hbm, mixer_gain_hbm, write_hbm, decay_hbm, rate_hbm, bias_hbm,
    head_gain_hbm, channel_gain_hbm, routes_hbm, route_weights_hbm,
    state_hbm, query_hbm, key_hbm, value_hbm, out_hbm,
    gate_hbm, up_hbm, down_hbm, sgate_hbm, sup_hbm, sdown_hbm,
    layer_ref, next_ref,
    tokens, mixer_gain, write_w, decay_w, rate, bias, head_gain, channel_gain,
    routes, route_weights, state, kqv_w, out_w, gu_w, down_w, sgu_w, sdown_w,
    normed, columns, keep_rows, step_rows, spread,
    wext, part_send, part_recv, residuals, own_residual, packed, wpacked,
    own_part, plane_send, plane_recv, line_send, line_recv,
    small_sems, kqv_sems, state_sem, out_sem, expert_sems, shared_sems,
    core_send_sems, core_recv_sems,
    wz_send_sems, wz_recv_sems, wy_send_sems, wy_recv_sems,
    part_send_sems, part_recv_sems, fwd_send_sems, fwd_recv_sems,
    plane_send_sems, plane_recv_sems, line_send_sems, line_recv_sems,
):
    rows, width = tokens.shape
    heads, dim = state.shape[1], state.shape[2]
    keys = heads * dim
    hidden = down_w.shape[0] // 2
    shidden = sdown_w.shape[0]
    share = width // tps
    me, tp = lax.axis_index("ep"), lax.axis_index("tp")
    core, chip = me % 2, me // 2
    y, z = chip % ys, chip // ys
    expert_total = 2 * ys * zs
    high_rows = round_up(rows, 8)

    def ep_of(dz, dy, dc):
        return (flip(z, dz) * ys + flip(y, dy)) * 2 + flip(core, dc)

    def local(src, dst, sem):
        copy = pltpu.make_async_copy(src, dst, sem)
        copy.start()
        return copy

    small = [
        local(src, dst, small_sems.at[i])
        for i, (src, dst) in enumerate((
            (tokens_hbm, tokens), (mixer_gain_hbm, mixer_gain), (write_hbm, write_w),
            (decay_hbm, decay_w), (rate_hbm, rate), (bias_hbm, bias),
            (head_gain_hbm, head_gain), (channel_gain_hbm, channel_gain),
            (routes_hbm, routes), (route_weights_hbm, route_weights),
        ))
    ]
    kqv = [
        local(src, kqv_w.at[:, i * keys : (i + 1) * keys], kqv_sems.at[i])
        for i, src in enumerate((key_hbm, query_hbm, value_hbm))
    ]
    state_load = local(state_hbm, state, state_sem)
    out_load = local(out_hbm, out_w, out_sem)

    peers = [(ep_of(dz, 0, 0), flip(tp, dt)) for dz in range(zs) for dt in range(tps) if dz or dt]
    peers += [(ep_of(0, dy, 0), flip(tp, dt)) for dy in range(1, ys) for dt in range(tps)]
    peers += [(ep_of(0, 0, 1), tp)]
    barrier = pltpu.get_barrier_semaphore()
    for peer in peers:
        pl.semaphore_signal(barrier, inc=1, device_id=peer, device_id_type=MESH)

    expert_loads = [
        local(src, dst, expert_sems.at[i])
        for i, (src, dst) in enumerate((
            (gate_hbm, gu_w.at[:, :hidden]), (up_hbm, gu_w.at[:, hidden : 2 * hidden]),
            (down_hbm, down_w.at[:hidden, :]),
        ))
    ]
    shared_loads = [
        local(src, dst, shared_sems.at[i])
        for i, (src, dst) in enumerate((
            (sgate_hbm, sgu_w.at[:, :shidden]), (sup_hbm, sgu_w.at[:, shidden:]),
            (sdown_hbm, sdown_w),
        ))
    ]

    sent = []

    def remote(src, dst, send_sem, recv_sem, peer):
        copy = pltpu.make_async_remote_copy(
            src_ref=src, dst_ref=dst, send_sem=send_sem, recv_sem=recv_sem,
            device_id=peer, device_id_type=MESH,
        )
        copy.start()
        sent.append(copy)
        return copy

    for copy in small:
        copy.wait()

    raw = route_weights[...]
    norm = raw / jnp.sum(raw, axis=0, keepdims=True) * ROUTED_SCALE
    named_all = routes[...]
    row = lax.broadcasted_iota(jnp.int32, (spread.shape[0], rows), 0)
    high = jnp.zeros(row.shape, F32)
    for k in range(named_all.shape[0]):
        named = named_all[k : k + 1, :]
        hit = (row == named) | (row == named + expert_total)
        high = high + jnp.where(hit, norm[k : k + 1, :], 0.0)
    rounded = high.astype(BF16).astype(F32)
    spread[:, :rows] = jnp.where(row < expert_total, rounded, high - rounded)
    wext[0] = spread[...].T[:rows, :].astype(BF16)

    tokens_wide = tokens[...].astype(F32)
    normed[rows // 16 * 16 :, :] = jnp.zeros((pad - rows // 16 * 16, width), BF16)
    normed[:rows, :] = rms_rows(tokens_wide, mixer_gain[...]).astype(BF16)
    wide = normed[...].astype(F32)[:high_rows, :]

    def per_head_dot(ref):
        table = ref[...].astype(F32)
        return [jnp.sum(wide * table[h : h + 1, :], axis=-1, keepdims=True) for h in range(heads)]

    write_rate = [jax.nn.sigmoid(x) for x in per_head_dot(write_w)]
    keep = []
    for h, pre in enumerate(per_head_dot(decay_w)):
        pre = pre + bias[:, h : h + 1]
        softplus = jnp.maximum(pre, 0.0) + jnp.log1p(jnp.exp(-jnp.abs(pre)))
        keep.append(jnp.exp(-rate[:, h : h + 1] * softplus))

    for copy in kqv:
        copy.wait()
    kqv_raw = jnp.dot(normed[...], kqv_w[...], preferred_element_type=F32).astype(BF16).astype(F32)

    pl.semaphore_wait(barrier, len(peers))
    sibling = (ep_of(0, 0, 1), tp)
    core_copies = [
        remote(src, dst, core_send_sems.at[i], core_recv_sems.at[i], sibling)
        for i, (src, dst) in enumerate((
            (gate_hbm, gu_w.at[:, 2 * hidden : 3 * hidden]),
            (up_hbm, gu_w.at[:, 3 * hidden :]),
            (down_hbm, down_w.at[hidden:, :]),
        ))
    ]

    def slot(dz, dy):
        return dz * ys + dy

    far_first = list(range(zs - 1, 0, -1))
    wz_copies = {
        dz: remote(wext.at[0], wext.at[slot(dz, 0)], wz_send_sems.at[dz], wz_recv_sems.at[dz],
                   (ep_of(dz, 0, 0), tp))
        for dz in far_first
    }

    heads_of = [slice(h * dim, (h + 1) * dim) for h in range(heads)]
    key_raw = [kqv_raw[:high_rows, :keys][:, part] for part in heads_of]
    query_raw = [kqv_raw[:high_rows, keys : 2 * keys][:, part] for part in heads_of]
    value_raw = [kqv_raw[:high_rows, 2 * keys :][:, part] for part in heads_of]
    state_load.wait()
    lane8 = lax.broadcasted_iota(jnp.int32, (8, dim), 0)
    seen = [[] for _ in range(heads)]
    asked = [[] for _ in range(heads)]
    for first in range(0, rows, 8):
        eight = slice(first, first + 8)
        left = jnp.concatenate(
            [x[eight] for h in range(heads) for x in (key_raw[h], query_raw[h])], axis=0
        ).astype(BF16)
        seen8 = [jnp.zeros((8, dim), F32)] * heads
        asked8 = [jnp.zeros((8, dim), F32)] * heads
        for r in range(first, min(first + 8, rows)):
            right = jnp.concatenate([state[r, h].astype(BF16) for h in range(heads)], axis=1)
            product = jnp.dot(left, right, preferred_element_type=F32)
            mine = lane8 == r - first
            for h in range(heads):
                block = product[h * 16 : (h + 1) * 16, heads_of[h]]
                seen8[h] = jnp.where(mine, block[:8], seen8[h])
                asked8[h] = jnp.where(mine, block[8:], asked8[h])
        for h in range(heads):
            seen[h].append(seen8[h])
            asked[h].append(asked8[h])

    head_out = []
    for h in range(heads):
        seen_h, asked_h = jnp.concatenate(seen[h], axis=0), jnp.concatenate(asked[h], axis=0)
        k_scale = lax.rsqrt(jnp.sum(key_raw[h] * key_raw[h], axis=-1, keepdims=True) + EPS)
        q_scale = lax.rsqrt(jnp.sum(query_raw[h] * query_raw[h], axis=-1, keepdims=True) + EPS)
        key_unit = key_raw[h] * k_scale
        query_unit = query_raw[h] * (q_scale * dim ** (-0.5))
        dots = jnp.sum(key_unit * query_unit, axis=-1, keepdims=True)
        step = write_rate[h] * (value_raw[h] - (keep[h] * k_scale) * seen_h)
        read = (keep[h] * q_scale * dim ** (-0.5)) * asked_h + dots * step
        head_out.append(rms_rows(read, head_gain[...]))
        columns[h * pad : h * pad + high_rows, :] = key_unit
        keep_rows[h] = jnp.broadcast_to(keep[h], (high_rows, dim))
        step_rows[h] = step

    out_load.wait()
    partial = jnp.dot(jnp.concatenate(head_out, axis=1).astype(BF16), out_w[...],
                      preferred_element_type=F32)[:rows]
    partial = partial + jnp.where(tp == 0, 1.0, 0.0) * tokens_wide
    for t in range(tps):
        part_send[t] = partial[:, t * share : (t + 1) * share].astype(BF16)
    part_copies = {}
    for dz in far_first + [0]:
        for dt in range(tps - 1, -1, -1):
            if dz or dt:
                at = dz * tps + dt
                part_copies[at] = remote(
                    part_send.at[flip(tp, dt)], part_recv.at[at],
                    part_send_sems.at[at], part_recv_sems.at[at], (ep_of(dz, 0, 0), flip(tp, dt)))

    turned = columns[...].T
    for r in range(rows):
        for h in range(heads):
            at = h * pad + r
            k_col = jnp.broadcast_to(turned[:, at : at + 1], (dim, dim))
            next_ref[r, h] = (keep_rows[h, r : r + 1, :] * state[r, h]
                              + k_col * step_rows[h, r : r + 1, :])

    wy_copies = {}

    def pass_weights(dz):
        if dz:
            wz_copies[dz].wait_recv()
        for dy in range(1, ys):
            at = slot(dz, dy)
            wy_copies[at] = remote(wext.at[slot(dz, 0)], wext.at[at], wy_send_sems.at[at],
                                   wy_recv_sems.at[at], (ep_of(0, dy, 0), tp))

    for dz in range(zs):
        pass_weights(dz)

    my_columns = pl.ds(pl.multiple_of(tp * share, 128), share)
    plane = [(dy, dt) for dy in range(ys) for dt in range(tps) if dy or dt]
    fwd_copies = {}

    def plane_at(dz, dy, dt):
        return (dz * ys + dy) * tps + dt

    def pass_residual(dz):
        total = part_send[tp].astype(F32) if dz == 0 else None
        for dt in range(tps):
            at = dz * tps + dt
            if at:
                part_copies[at].wait_recv()
                piece = part_recv[at].astype(F32)
                total = piece if total is None else total + piece
        residual = total.astype(BF16)
        if dz == 0:
            own_residual[...] = residual.astype(F32)
        residuals[slot(dz, 0), :, my_columns] = residual
        for dy, dt in reversed(plane):
            at = plane_at(dz, dy, dt)
            fwd_copies[at] = remote(
                residuals.at[slot(dz, 0), :, my_columns], residuals.at[slot(dz, dy), :, my_columns],
                fwd_send_sems.at[at], fwd_recv_sems.at[at], (ep_of(0, dy, 0), flip(tp, dt)))

    def gated(product, half):
        g, u = product[:, :half], product[:, half : 2 * half]
        return g * jax.nn.sigmoid(g) * u

    plane_copies = {}

    def run_chunk(dz):
        for dy, dt in plane:
            fwd_copies[plane_at(dz, dy, dt)].wait_recv()
        for dy in range(ys):
            if dy:
                wy_copies[slot(dz, dy)].wait_recv()
            at = dy * pad
            packed[at : at + rows, :] = rms_rows(
                residuals[slot(dz, dy)].astype(F32), channel_gain[...]).astype(BF16)
            wpacked[at : at + rows, :] = wext[slot(dz, dy)]
        x = packed[...]
        product = jnp.dot(x, gu_w[...], preferred_element_type=F32)
        weights = wpacked[...].astype(F32)
        lane = lax.broadcasted_iota(jnp.int32, weights.shape, 1)
        acts = []
        for e in range(2):
            expert = flip(me, e)
            mine = (lane == expert) | (lane == expert + expert_total)
            scale = jnp.sum(jnp.where(mine, weights, 0.0), axis=1, keepdims=True)
            acts.append((gated(product[:, 2 * e * hidden : (2 * e + 2) * hidden], hidden)
                         * scale).astype(BF16))
        down = jnp.dot(jnp.concatenate(acts, axis=1), down_w[...], preferred_element_type=F32)
        own = down[:rows]
        if dz == 0:
            shared_act = gated(jnp.dot(packed[:pad, :], sgu_w[...], preferred_element_type=F32),
                               shidden).astype(BF16)
            own = own + jnp.dot(shared_act, sdown_w[...], preferred_element_type=F32)[:rows]
        for t in range(tps):
            own_part[dz * tps + t] = own[:, t * share : (t + 1) * share]
        for dy in range(ys):
            block = own if dy == 0 else down[dy * pad : dy * pad + rows]
            for t in range(tps):
                plane_send[plane_at(dz, dy, t)] = block[:, t * share : (t + 1) * share].astype(BF16)
        for dy, dt in reversed(plane):
            at = plane_at(dz, dy, dt)
            plane_copies[at] = remote(
                plane_send.at[plane_at(dz, dy, 0) + flip(tp, dt)], plane_recv.at[at],
                plane_send_sems.at[at], plane_recv_sems.at[at], (ep_of(0, dy, 0), flip(tp, dt)))

    line_copies = {}

    def plane_sum(dz):
        total = own_part[dz * tps + tp]
        for dy, dt in plane:
            at = plane_at(dz, dy, dt)
            plane_copies[at].wait_recv()
            total = total + plane_recv[at].astype(F32)
        return total

    def return_line(dz):
        line_send[dz] = plane_sum(dz).astype(BF16)
        line_copies[dz] = remote(line_send.at[dz], line_recv.at[dz], line_send_sems.at[dz],
                                 line_recv_sems.at[dz], (ep_of(dz, 0, 0), tp))

    for dz in range(zs):
        pass_residual(dz)
    for copy in expert_loads + shared_loads:
        copy.wait()
    for copy in core_copies:
        copy.wait_recv()
    for dz in range(zs):
        run_chunk(dz)
    for dz in range(1, zs):
        return_line(dz)
    result = own_residual[...] + plane_sum(0)
    for dz in range(1, zs):
        line_copies[dz].wait_recv()
        result = result + line_recv[dz].astype(F32)
    layer_ref[...] = result.astype(BF16)
    for copy in sent:
        copy.wait_send()


def store_kernel(layer_ref, next_ref, layer_hbm, next_hbm, sems):
    copies = [
        pltpu.make_async_copy(next_ref, next_hbm, sems.at[0]),
        pltpu.make_async_copy(layer_ref, layer_hbm, sems.at[1]),
    ]
    for copy in copies:
        copy.start()
    for copy in copies:
        copy.wait()


def per_device(
    ep_count, tp_count,
    tokens, delta_state, mixer_gain, query_weight, key_weight, value_weight,
    write_weight, decay_weight, decay_rate, decay_bias, head_gain, out_weight,
    channel_gain, routes, route_weights, expert_gate, expert_up, expert_down,
    shared_gate, shared_up, shared_down,
):
    rows, width = tokens.shape
    heads, dim = delta_state.shape[1], delta_state.shape[2]
    hidden = expert_gate.shape[2]
    shidden = shared_gate.shape[1]
    keys = heads * dim
    top = routes.shape[1]
    chips = ep_count // 2
    ys = 1
    while 4 * ys * ys <= chips:
        ys *= 2
    zs = chips // ys
    extra = round_up(2 * ep_count, 128)
    share = width // tp_count
    pad = round_up(rows, 16)
    high_rows = round_up(rows, 8)
    zy, zt, zyt = zs * ys, zs * tp_count, zs * ys * tp_count
    vmem = pl.BlockSpec(memory_space=pltpu.VMEM)
    hbm = pl.BlockSpec(memory_space=pltpu.HBM)
    dma = pltpu.SemaphoreType.DMA

    layer_out, next_state = pl.pallas_call(
        functools.partial(layer_kernel, zs, ys, tp_count, pad),
        out_shape=(pltpu.VMEM((rows, share), BF16), pltpu.VMEM(delta_state.shape, F32)),
        in_specs=[hbm] * 21,
        out_specs=(vmem, vmem),
        scratch_shapes=[
            pltpu.VMEM((rows, width), BF16), pltpu.VMEM((1, width), F32),
            pltpu.VMEM((heads, width), BF16), pltpu.VMEM((heads, width), BF16),
            pltpu.VMEM((1, heads), F32), pltpu.VMEM((1, heads), F32),
            pltpu.VMEM((1, dim), F32), pltpu.VMEM((1, width), F32),
            pltpu.VMEM((top, rows), jnp.int32), pltpu.VMEM((top, rows), F32),
            pltpu.VMEM(delta_state.shape, F32),
            pltpu.VMEM((width, 3 * keys), BF16), pltpu.VMEM((keys, width), BF16),
            pltpu.VMEM((width, 4 * hidden), BF16), pltpu.VMEM((2 * hidden, width), BF16),
            pltpu.VMEM((width, 2 * shidden), BF16), pltpu.VMEM((shidden, width), BF16),
            pltpu.VMEM((pad, width), BF16),
            pltpu.VMEM((round_up(heads * pad, 128), dim), F32),
            pltpu.VMEM((heads, high_rows, dim), F32), pltpu.VMEM((heads, high_rows, dim), F32),
            pltpu.VMEM((extra, round_up(rows, 128)), F32),
            pltpu.VMEM((zy, rows, extra), BF16),
            pltpu.VMEM((tp_count, rows, share), BF16), pltpu.VMEM((zt, rows, share), BF16),
            pltpu.VMEM((zy, rows, width), BF16), pltpu.VMEM((rows, share), F32),
            pltpu.VMEM((ys * pad, width), BF16), pltpu.VMEM((ys * pad, extra), BF16),
            pltpu.VMEM((zt, rows, share), F32),
            pltpu.VMEM((zyt, rows, share), BF16), pltpu.VMEM((zyt, rows, share), BF16),
            pltpu.VMEM((zs, rows, share), BF16), pltpu.VMEM((zs, rows, share), BF16),
            dma((10,)), dma((3,)), dma, dma, dma((3,)), dma((3,)),
            dma((3,)), dma((3,)),
            dma((zs,)), dma((zs,)), dma((zy,)), dma((zy,)),
            dma((zt,)), dma((zt,)), dma((zyt,)), dma((zyt,)),
            dma((zyt,)), dma((zyt,)), dma((zs,)), dma((zs,)),
        ],
        compiler_params=pltpu.CompilerParams(
            collective_id=0, has_side_effects=True, vmem_limit_bytes=44 * 2**20),
    )(
        *[x if x.size == 1 else pltpu.with_memory_space_constraint(x, pltpu.HBM) for x in (
            tokens, mixer_gain.reshape(1, width), write_weight.T, decay_weight.T,
            decay_rate.reshape(1, heads), decay_bias.reshape(1, heads), head_gain.reshape(1, dim),
            channel_gain.reshape(1, width), routes.T, route_weights.T,
            delta_state, query_weight, key_weight, value_weight, out_weight,
            expert_gate.reshape(width, hidden), expert_up.reshape(width, hidden),
            expert_down.reshape(hidden, width), shared_gate, shared_up, shared_down,
        )]
    )
    return pl.pallas_call(
        store_kernel,
        out_shape=(
            jax.ShapeDtypeStruct(layer_out.shape, BF16),
            jax.ShapeDtypeStruct(delta_state.shape, F32),
        ),
        in_specs=[vmem, vmem],
        out_specs=(hbm, hbm),
        scratch_shapes=[dma((2,))],
        compiler_params=pltpu.CompilerParams(vmem_limit_bytes=8 * 2**20),
    )(layer_out, next_state)


def solution(mesh):
    return jax.shard_map(
        functools.partial(per_device, mesh.shape["ep"], mesh.shape["tp"]),
        mesh=mesh,
        in_specs=(
            P("ep", None),
            P("ep", "tp", None, None),
            P(),
            P(None, "tp"),
            P(None, "tp"),
            P(None, "tp"),
            P(None, "tp"),
            P(None, "tp"),
            P("tp"),
            P("tp"),
            P(),
            P("tp", None),
            P(),
            P("ep", None),
            P("ep", None),
            P("ep", None, "tp"),
            P("ep", None, "tp"),
            P("ep", "tp", None),
            P(None, "tp"),
            P(None, "tp"),
            P("tp", None),
        ),
        out_specs=(P("ep", "tp"), P("ep", "tp", None, None)),
        check_vma=False,
    )
```

time: 41.1 us -> 29.4 us (0.72)
  Pallas kernels: 38.8 us -> 28.6 us
  local copies, waits for them, and re-layouts: 1.35 us -> 0 us
    pallas_call x2, Pallas kernels: 38.8 us -> 28.6 us  [the longest x1 27.2 us: per_device(): pl.pallas_call(functools.partial(layer_kernel, zs, ys, tp_count, pad), ou...]
    unnamed x1 -> x0, local copies, waits for them, and re-layouts: 1.35 us -> none
where the time goes in v1:
time: 29.4 us; the launch traced here: 29.2 us
  Pallas kernels  28.6 us (97%)
  between operations  0.65 us (2%)
    pallas_call x1, Pallas kernels, per_device(): pl.pallas_call(functools.partial(layer_kernel, zs, ys, tp_count, pad), ou...  27.2 us
    pallas_call x1, Pallas kernels, per_device(): pl.pallas_call(store_kernel, out_shape=(jax.ShapeDtypeStruct(layer_out.sh...  1.43 us

profile of v1, /device:TPU:0, one launch (start us, length us, event | category | flops | bytes accessed | tf_op | source)
XLA Modules:
  0.0 29.2 jit_solution(9867406228444738639)
XLA Ops:
  0.6 27.2 %shard_map.212 = (bf16[18,512]{1,0:T(8,128)(2,1)S(1)}, f32[18,2,128,128]{3,2,1,0:T(8,128)S(1)}) custom-call(bf16[18,1024]{1,0:T(8,128)(2,1)} %tokens_hbm.1, f32[1,1024]{1,0:T(1,128)} %bitcast.15, bf16[2,1024]{1,0:T(2,128)(2,1)} %bitcast.16, bf16[2,1024]{1,0:T(2,128)(2,1)} %bitcast.17, f32[1,2]{1,0:T(1,128)} %bitcast.21, f32[1,2]{1,0:T(1,128)} %bitcast.22, ...), custom_call_target="tpu_custom_call" | custom-call | tf_op jit(solution)/shard_map/pallas_call | solution.py:399
  27.8 1.4 %shard_map.213 = (bf16[18,512]{1,0:T(8,128)(2,1)}, f32[18,2,128,128]{3,2,1,0:T(8,128)}) custom-call(bf16[18,512]{1,0:T(8,128)(2,1)S(1)} %get-tuple-element.4.layer_ref, f32[18,2,128,128]{3,2,1,0:T(8,128)S(1)} %get-tuple-element.5.next_ref), custom_call_target="tpu_custom_call" | custom-call | tf_op jit(solution)/shard_map/pallas_call | solution.py:443

commit v2 on v1

--- a/solution.py
+++ b/solution.py
@@ -93,21 +93,6 @@
     for peer in peers:
         pl.semaphore_signal(barrier, inc=1, device_id=peer, device_id_type=MESH)
 
-    expert_loads = [
-        local(src, dst, expert_sems.at[i])
-        for i, (src, dst) in enumerate((
-            (gate_hbm, gu_w.at[:, :hidden]), (up_hbm, gu_w.at[:, hidden : 2 * hidden]),
-            (down_hbm, down_w.at[:hidden, :]),
-        ))
-    ]
-    shared_loads = [
-        local(src, dst, shared_sems.at[i])
-        for i, (src, dst) in enumerate((
-            (sgate_hbm, sgu_w.at[:, :shidden]), (sup_hbm, sgu_w.at[:, shidden:]),
-            (sdown_hbm, sdown_w),
-        ))
-    ]
-
     sent = []
 
     def remote(src, dst, send_sem, recv_sem, peer):
@@ -155,32 +140,30 @@
         copy.wait()
     kqv_raw = jnp.dot(normed[...], kqv_w[...], preferred_element_type=F32).astype(BF16).astype(F32)
 
-    pl.semaphore_wait(barrier, len(peers))
-    sibling = (ep_of(0, 0, 1), tp)
-    core_copies = [
-        remote(src, dst, core_send_sems.at[i], core_recv_sems.at[i], sibling)
-        for i, (src, dst) in enumerate((
-            (gate_hbm, gu_w.at[:, 2 * hidden : 3 * hidden]),
-            (up_hbm, gu_w.at[:, 3 * hidden :]),
-            (down_hbm, down_w.at[hidden:, :]),
-        ))
-    ]
-
     def slot(dz, dy):
         return dz * ys + dy
 
     far_first = list(range(zs - 1, 0, -1))
-    wz_copies = {
-        dz: remote(wext.at[0], wext.at[slot(dz, 0)], wz_send_sems.at[dz], wz_recv_sems.at[dz],
-                   (ep_of(dz, 0, 0), tp))
-        for dz in far_first
-    }
-
     heads_of = [slice(h * dim, (h + 1) * dim) for h in range(heads)]
     key_raw = [kqv_raw[:high_rows, :keys][:, part] for part in heads_of]
     query_raw = [kqv_raw[:high_rows, keys : 2 * keys][:, part] for part in heads_of]
     value_raw = [kqv_raw[:high_rows, 2 * keys :][:, part] for part in heads_of]
     state_load.wait()
+    expert_loads = [
+        local(src, dst, expert_sems.at[i])
+        for i, (src, dst) in enumerate((
+            (gate_hbm, gu_w.at[:, :hidden]), (up_hbm, gu_w.at[:, hidden : 2 * hidden]),
+            (down_hbm, down_w.at[:hidden, :]),
+        ))
+    ]
+    shared_loads = [
+        local(src, dst, shared_sems.at[i])
+        for i, (src, dst) in enumerate((
+            (sgate_hbm, sgu_w.at[:, :shidden]), (sup_hbm, sgu_w.at[:, shidden:]),
+            (sdown_hbm, sdown_w),
+        ))
+    ]
+
     lane8 = lax.broadcasted_iota(jnp.int32, (8, dim), 0)
     seen = [[] for _ in range(heads)]
     asked = [[] for _ in range(heads)]
@@ -224,6 +207,13 @@
     partial = partial + jnp.where(tp == 0, 1.0, 0.0) * tokens_wide
     for t in range(tps):
         part_send[t] = partial[:, t * share : (t + 1) * share].astype(BF16)
+    pl.semaphore_wait(barrier, len(peers))
+    wz_copies = {
+        dz: remote(wext.at[0], wext.at[slot(dz, 0)], wz_send_sems.at[dz], wz_recv_sems.at[dz],
+                   (ep_of(dz, 0, 0), tp))
+        for dz in far_first
+    }
+
     part_copies = {}
     for dz in far_first + [0]:
         for dt in range(tps - 1, -1, -1):
@@ -233,6 +223,16 @@
                     part_send.at[flip(tp, dt)], part_recv.at[at],
                     part_send_sems.at[at], part_recv_sems.at[at], (ep_of(dz, 0, 0), flip(tp, dt)))
 
+    sibling = (ep_of(0, 0, 1), tp)
+    core_copies = [
+        remote(src, dst, core_send_sems.at[i], core_recv_sems.at[i], sibling)
+        for i, (src, dst) in enumerate((
+            (gate_hbm, gu_w.at[:, 2 * hidden : 3 * hidden]),
+            (up_hbm, gu_w.at[:, 3 * hidden :]),
+            (down_hbm, down_w.at[hidden:, :]),
+        ))
+    ]
+
     turned = columns[...].T
     for r in range(rows):
         for h in range(heads):
@@ -250,9 +250,6 @@
             at = slot(dz, dy)
             wy_copies[at] = remote(wext.at[slot(dz, 0)], wext.at[at], wy_send_sems.at[at],
                                    wy_recv_sems.at[at], (ep_of(0, dy, 0), tp))
-
-    for dz in range(zs):
-        pass_weights(dz)
 
     my_columns = pl.ds(pl.multiple_of(tp * share, 128), share)
     plane = [(dy, dt) for dy in range(ys) for dt in range(tps) if dy or dt]
@@ -339,18 +336,19 @@
         line_copies[dz] = remote(line_send.at[dz], line_recv.at[dz], line_send_sems.at[dz],
                                  line_recv_sems.at[dz], (ep_of(dz, 0, 0), tp))
 
-    for dz in range(zs):
+    for dz in [0] + far_first:
         pass_residual(dz)
+        pass_weights(dz)
     for copy in expert_loads + shared_loads:
         copy.wait()
     for copy in core_copies:
         copy.wait_recv()
-    for dz in range(zs):
+    for dz in far_first + [0]:
         run_chunk(dz)
-    for dz in range(1, zs):
+    for dz in far_first:
         return_line(dz)
     result = own_residual[...] + plane_sum(0)
-    for dz in range(1, zs):
+    for dz in far_first:
         line_copies[dz].wait_recv()
         result = result + line_recv[dz].astype(F32)
     layer_ref[...] = result.astype(BF16)

time: 29.4 us -> 28.5 us (0.969)
  Pallas kernels: 28.6 us -> 27.7 us
    pallas_call x1, Pallas kernels: 27.2 us -> 26.2 us  [per_device(): pl.pallas_call(functools.partial(layer_kernel, zs, ys, tp_count, pad), ou...]
where the time goes in v2:
time: 28.5 us; the launch traced here: 28.3 us
  Pallas kernels  27.7 us (97%)
  between operations  0.65 us (2%)
    pallas_call x1, Pallas kernels, per_device(): pl.pallas_call(functools.partial(layer_kernel, zs, ys, tp_count, pad), ou...  26.2 us
    pallas_call x1, Pallas kernels, per_device(): pl.pallas_call(store_kernel, out_shape=(jax.ShapeDtypeStruct(layer_out.sh...  1.43 us

profile of v2, /device:TPU:0, one launch (start us, length us, event | category | flops | bytes accessed | tf_op | source)
XLA Modules:
  0.0 28.3 jit_solution(5529851604321444292)
XLA Ops:
  0.6 26.2 %shard_map.212 = (bf16[18,512]{1,0:T(8,128)(2,1)S(1)}, f32[18,2,128,128]{3,2,1,0:T(8,128)S(1)}) custom-call(bf16[18,1024]{1,0:T(8,128)(2,1)} %tokens_hbm.1, f32[1,1024]{1,0:T(1,128)} %bitcast.15, bf16[2,1024]{1,0:T(2,128)(2,1)} %bitcast.16, bf16[2,1024]{1,0:T(2,128)(2,1)} %bitcast.17, f32[1,2]{1,0:T(1,128)} %bitcast.21, f32[1,2]{1,0:T(1,128)} %bitcast.22, ...), custom_call_target="tpu_custom_call" | custom-call | tf_op jit(solution)/shard_map/pallas_call | solution.py:397
  26.9 1.4 %shard_map.213 = (bf16[18,512]{1,0:T(8,128)(2,1)}, f32[18,2,128,128]{3,2,1,0:T(8,128)}) custom-call(bf16[18,512]{1,0:T(8,128)(2,1)S(1)} %get-tuple-element.4.layer_ref, f32[18,2,128,128]{3,2,1,0:T(8,128)S(1)} %get-tuple-element.5.next_ref), custom_call_target="tpu_custom_call" | custom-call | tf_op jit(solution)/shard_map/pallas_call | solution.py:441
